TPU v7x, 32 devices: a whole 2x2x4 slice. The times are simulated.
32 devices in a mesh: rep: 2 (over x), fs: 8 (over z, y), tp: 2 (over core).
Axes of the slice: x: 2, y: 2, z: 4, core: 2. Of those that a mesh axis runs over, the one named last changes fastest.
Arguments:
- tokens: bfloat16 [12288, 2048], P(('rep', 'fs'), 'tp'), may hold values from -6 to 6
- first_norm_gain: bfloat16 [2048], replicated, may hold values from 0.099609375 to 1.8984375
- query_projection_weight: bfloat16 [2048, 512], P('fs', 'tp'), may hold values from -0.125 to 0.125
- key_projection_weight: bfloat16 [2048, 512], P('fs', 'tp'), may hold values from -0.125 to 0.125
- value_projection_weight: bfloat16 [2048, 1024], P('fs', 'tp'), may hold values from -0.125 to 0.125
- output_gate_weight: bfloat16 [2048, 1024], P('fs', 'tp'), may hold values from -0.125 to 0.125
- decay_projection_weight: bfloat16 [2048, 512], P('fs', 'tp'), may hold values from -0.375 to 0.375
- fading_shift_vector: float32 [512], P('tp'), may hold values from -1 to 4
- added_fading_exponent: float32 [12288, 512], P(('rep', 'fs'), 'tp'), may hold values from -0.7 to 0
- per_head_gain: bfloat16 [128], replicated, may hold values from 0.099609375 to 1.8984375
- mixer_result_matrix: bfloat16 [1024, 2048], P('tp', 'fs'), may hold values from -0.1875 to 0.1875
- second_norm_gain: bfloat16 [2048], replicated, may hold values from 0.099609375 to 1.8984375
- up_linear_weight: bfloat16 [2048, 3072], P('fs', 'tp'), may hold values from -0.125 to 0.125
- up_gating_weight: bfloat16 [2048, 3072], P('fs', 'tp'), may hold values from -0.125 to 0.125
- depthwise_taps: bfloat16 [2, 3, 3072], P(None, None, 'tp'), may hold values from -3.5 to 3.5
- depthwise_bias: bfloat16 [2, 3072], P(None, 'tp'), may hold values from -3 to 3
- down_projection_weight: bfloat16 [3072, 2048], P('tp', 'fs'), may hold values from -0.109375 to 0.109375
Outputs:
- mixed: bfloat16 [12288, 2048], P(('rep', 'fs'), 'tp')
All inputs are finite; a program needn't handle non-finite values.
Results may differ from a plain program's by a relative error of at most 0.018.
Values may be sent and summed in bfloat16 or wider, within the bound.
A program may use at most 128 MiB of HBM per device.

v0:
```python
import jax
import jax.numpy as jnp
from jax import lax
from jax.sharding import PartitionSpec as P

KEY_DIM = 64
VALUE_DIM = 128
BLOCK = 64
SEQ_LEN = 256


norm_eps = 1e-06
fading_sharpness = 16.0


def normalize(source, gain):
    widened = source.astype(jnp.float32)
    scaled = widened * lax.rsqrt(jnp.mean(widened * widened, axis=-1, keepdims=True) + norm_eps)
    return (scaled * gain.astype(jnp.float32)).astype(jnp.bfloat16)


def direction(queries, key_heads, value_heads, fading_exponent):
    sequences, length, head_count, key_depth = queries.shape
    value_depth = value_heads.shape[-1]
    block_count = length // BLOCK
    query_blocks = queries.reshape(sequences, block_count, BLOCK, head_count, key_depth)
    key_blocks = key_heads.reshape(sequences, block_count, BLOCK, head_count, key_depth)
    value_blocks = value_heads.reshape(sequences, block_count, BLOCK, head_count, value_depth)
    cumulative = jnp.cumsum(
        fading_exponent.reshape(sequences, block_count, BLOCK, head_count, key_depth), axis=2
    )
    block_total = cumulative[:, :, -1:]
    query_decayed = query_blocks * jnp.exp(cumulative)
    key_inverse = key_blocks * jnp.exp(-cumulative)
    key_carried = key_blocks * jnp.exp(block_total - cumulative)
    lower_mask = jnp.tril(jnp.ones((BLOCK, BLOCK), dtype=bool))
    scores = jnp.einsum(
        "snihd,snjhd->snhij", query_decayed, key_inverse, precision=lax.Precision.HIGHEST
    )
    scores = jnp.where(lower_mask, scores, 0.0)
    within_block = jnp.einsum(
        "snhij,snjhv->snihv", scores, value_blocks, precision=lax.Precision.HIGHEST
    )
    increments = jnp.einsum(
        "snchd,snchv->nshdv", key_carried, value_blocks, precision=lax.Precision.HIGHEST
    )
    carry_decay = jnp.moveaxis(jnp.exp(block_total[:, :, 0]), 1, 0)

    def advance(running, inputs):
        factor, update = inputs
        return (factor[..., None] * running + update, running)

    initial = jnp.zeros((sequences, head_count, key_depth, value_depth), jnp.float32)
    unused, previous = lax.scan(advance, initial, (carry_decay, increments))
    across_blocks = jnp.einsum(
        "snchd,nshdv->snchv", query_decayed, previous, precision=lax.Precision.HIGHEST
    )
    return (within_block + across_blocks).reshape(sequences, length, head_count, value_depth)


def mixer_heads(queries_raw, keys_raw, values_raw, gates_raw, fading_exponent, per_head_gain):
    row_count = queries_raw.shape[0]
    head_count = values_raw.shape[1] // VALUE_DIM
    key_shape = (row_count // SEQ_LEN, SEQ_LEN, head_count, KEY_DIM)
    value_shape = (row_count // SEQ_LEN, SEQ_LEN, head_count, VALUE_DIM)
    queries = queries_raw.astype(jnp.float32).reshape(key_shape) * KEY_DIM ** (-0.5)
    key_heads = keys_raw.astype(jnp.float32).reshape(key_shape)
    value_heads = values_raw.astype(jnp.float32).reshape(value_shape)
    decay_heads = fading_exponent.reshape(key_shape)
    forward = direction(queries, key_heads, value_heads, decay_heads)
    backward = direction(
        jnp.flip(queries, 1),
        jnp.flip(key_heads, 1),
        jnp.flip(value_heads, 1),
        jnp.flip(decay_heads, 1),
    )
    attention = forward + jnp.flip(backward, 1)
    scaled = attention * lax.rsqrt(
        jnp.mean(attention * attention, axis=-1, keepdims=True) + norm_eps
    )
    scaled = scaled * per_head_gain.astype(jnp.float32)
    merged = scaled.reshape(row_count, head_count * VALUE_DIM)
    return (merged * jax.nn.silu(gates_raw.astype(jnp.float32))).astype(jnp.bfloat16)


def depthwise(linear_out, gated_out, depthwise_taps, depthwise_bias):
    row_count, channels = linear_out.shape

    def smooth(source, taps, offset_bias):
        framed = source.astype(jnp.float32).reshape(row_count // SEQ_LEN, SEQ_LEN, channels)
        tap_count = taps.shape[0]
        leading_zero_fill = tap_count // 2
        padded = jnp.pad(
            framed, ((0, 0), (leading_zero_fill, tap_count - 1 - leading_zero_fill), (0, 0))
        )
        result = offset_bias.astype(jnp.float32)
        for shift_index in range(tap_count):
            result = result + padded[:, shift_index : shift_index + SEQ_LEN] * taps[
                shift_index
            ].astype(jnp.float32)
        return result

    linear_conv = smooth(linear_out, depthwise_taps[0], depthwise_bias[0])
    gate_conv = smooth(gated_out, depthwise_taps[1], depthwise_bias[1])
    return (linear_conv * jax.nn.silu(gate_conv)).astype(jnp.bfloat16).reshape(row_count, channels)


def fold_rows(source, weight_pieces):
    return tuple(
        (
            jnp.dot(source, weight_piece, preferred_element_type=jnp.float32)
            for weight_piece in weight_pieces
        )
    )


def emit_with(source, weight_piece):
    return jnp.dot(source, weight_piece, preferred_element_type=jnp.float32)


def local(
    tokens,
    first_norm_gain,
    query_projection_weight,
    key_projection_weight,
    value_projection_weight,
    output_gate_weight,
    decay_projection_weight,
    fading_shift_vector,
    added_fading_exponent,
    per_head_gain,
    mixer_result_matrix,
    second_norm_gain,
    up_linear_weight,
    up_gating_weight,
    depthwise_taps,
    depthwise_bias,
    down_projection_weight,
):
    whole_rows = lax.all_gather(tokens, "tp", axis=1, tiled=True)
    normed = normalize(whole_rows, first_norm_gain)
    mapped_token_matrix = fold_rows(
        normed,
        (
            lax.all_gather(query_projection_weight, "fs", axis=0, tiled=True),
            lax.all_gather(key_projection_weight, "fs", axis=0, tiled=True),
            lax.all_gather(value_projection_weight, "fs", axis=0, tiled=True),
            lax.all_gather(output_gate_weight, "fs", axis=0, tiled=True),
            lax.all_gather(decay_projection_weight, "fs", axis=0, tiled=True),
        ),
    )
    queries_raw = mapped_token_matrix[0].astype(jnp.bfloat16)
    keys_raw = mapped_token_matrix[1].astype(jnp.bfloat16)
    values_raw = mapped_token_matrix[2].astype(jnp.bfloat16)
    gates_raw = mapped_token_matrix[3].astype(jnp.bfloat16)
    fading_exponent = (
        jax.nn.log_sigmoid(mapped_token_matrix[4] + fading_shift_vector) / fading_sharpness
        + added_fading_exponent
    )
    mixed_heads = mixer_heads(
        queries_raw, keys_raw, values_raw, gates_raw, fading_exponent, per_head_gain
    )
    mixer_terms = emit_with(
        mixed_heads, lax.all_gather(mixer_result_matrix, "fs", axis=1, tiled=True)
    )
    feature_share = tokens.shape[1]
    summed = lax.psum(mixer_terms.astype(jnp.bfloat16), "tp").astype(jnp.float32)
    full_after = (whole_rows.astype(jnp.float32) + summed).astype(jnp.bfloat16)
    after_mixer = lax.dynamic_slice_in_dim(
        full_after, lax.axis_index("tp") * feature_share, feature_share, 1
    )
    normed_two = normalize(full_after, second_norm_gain)
    upward = fold_rows(
        normed_two,
        (
            lax.all_gather(up_linear_weight, "fs", axis=0, tiled=True),
            lax.all_gather(up_gating_weight, "fs", axis=0, tiled=True),
        ),
    )
    linear_out = upward[0].astype(jnp.bfloat16)
    gated_out = upward[1].astype(jnp.bfloat16)
    hidden = depthwise(linear_out, gated_out, depthwise_taps, depthwise_bias)
    channel_terms = emit_with(
        hidden, lax.all_gather(down_projection_weight, "fs", axis=1, tiled=True)
    )
    channel_part = lax.psum_scatter(
        channel_terms.astype(jnp.bfloat16), "tp", scatter_dimension=1, tiled=True
    ).astype(jnp.float32)
    return (after_mixer.astype(jnp.float32) + channel_part).astype(jnp.bfloat16)


def solution(mesh):
    return jax.shard_map(
        local,
        mesh=mesh,
        in_specs=(
            P(("rep", "fs"), "tp"),
            P(),
            P("fs", "tp"),
            P("fs", "tp"),
            P("fs", "tp"),
            P("fs", "tp"),
            P("fs", "tp"),
            P("tp"),
            P(("rep", "fs"), "tp"),
            P(),
            P("tp", "fs"),
            P(),
            P("fs", "tp"),
            P("fs", "tp"),
            P(None, None, "tp"),
            P(None, "tp"),
            P("tp", "fs"),
        ),
        out_specs=P(("rep", "fs"), "tp"),
        check_vma=False,
    )
```

profile of v0, /device:TPU:25, one launch (start us, length us, event | category | flops | bytes accessed | tf_op | source)
XLA Modules:
  0.0 658.2 jit_solution(8518647654533081212)
XLA Ops:
  11.8 10.9 %all-gather.11.cloned.1.call-done = bf16[768,2048]{1,0:T(8,128)(2,1)} async-done(((bf16[768,1024]{1,0:T(8,128)(2,1)}), bf16[768,2048]{1,0:T(8,128)(2,1)}) %all-gather.11.cloned.1.call-update) | async-done | bytes 3145744 | tf_op jit(solution)/shard_map/all_gather | solution.py:140
  22.7 2.6 fusion.3
  25.3 37.0 %all-gather.17.cloned.1.call-done = bf16[2048,256]{1,0:T(8,128)(2,1)} async-done(((bf16[256,256]{1,0:T(8,128)(2,1)}), bf16[2048,256]{1,0:T(8,128)(2,1)}) %all-gather.17.cloned.1.call-update) | async-done | bytes 1048592 | tf_op jit(solution)/shard_map/all_gather | solution.py:149
  62.3 3.6 fusion.42
  68.3 35.2 %all-gather.19.cloned.1.call-done = bf16[2048,256]{1,0:T(8,128)(2,1)} async-done(((bf16[256,256]{1,0:T(8,128)(2,1)}), bf16[2048,256]{1,0:T(8,128)(2,1)}) %all-gather.19.cloned.1.call-update) | async-done | bytes 1048592 | tf_op jit(solution)/shard_map/all_gather | solution.py:146
  103.4 3.2 fusion.36
  106.6 1.8 reshape_reshape.11
  110.0 1.3 rev.19
  114.3 30.1 %all-gather.15.cloned.1.call-done = bf16[2048,256]{1,0:T(8,128)(2,1)} async-done(((bf16[256,256]{1,0:T(8,128)(2,1)}), bf16[2048,256]{1,0:T(8,128)(2,1)}) %all-gather.15.cloned.1.call-update) | async-done | bytes 1048592 | tf_op jit(solution)/shard_map/all_gather | solution.py:145
  144.4 3.2 broadcast_multiply_fusion.1
  147.6 1.8 mul.209
  151.3 1.6 copy.100
  153.3 1.3 rev.20
  154.6 2.1 copy.87
  156.7 4.9 exponential_multiply_fusion.3
  161.6 3.8 fusion.20
  165.4 2.6 exponential_multiply_fusion.1
  169.2 3.8 fusion.16
  173.0 22.6 %all-gather.13.cloned.1.call-done = bf16[2048,512]{1,0:T(8,128)(2,1)} async-done(((bf16[256,512]{1,0:T(8,128)(2,1)}), bf16[2048,512]{1,0:T(8,128)(2,1)}) %all-gather.13.cloned.1.call-update) | async-done | bytes 2097168 | tf_op jit(solution)/shard_map/all_gather | solution.py:147
  195.5 5.3 convolution_convert_fusion.5
  200.8 1.7 reshape_reshape.9
  202.6 2.8 reshape.131
  205.3 4.1 fusion.18
  210.8 8.1 %while.26 = (s32[]{:T(128)}, f32[3,4,64,128]{3,2,1,0:T(8,128)S(1)}, f32[4,3,4,64,128]{4,3,2,0,1:T(8,128)}, f32[4,3,4,64]{3,2,0,1:T(4,128)S(1)}, f32[4,3,4,64,128]{4,3,2,1,0:T(8,128)}, /*index=5*/s32[]{:T(128)}, s32[]{:T(128)}) while((s32[]{:T(128)}, f32[3,4,64,128]{3,2,1,0:T(8,128)S(1)}, f32[4,3,4,64,128]{4,3,2,0,1:T(8,128)}, ...), condition=%wide.region_3.4_spmd.clone, body=%wide.region_2.3_spmd.clone.sunk | while | flops 393219 | bytes 1975904 | solution.py:54
  219.0 2.5 fusion.23
  221.5 1.7 add_bitcast_fusion.1
  225.9 10.2 %rev.17 = f32[3,256,4,128]{3,1,2,0:T(8,128)S(1)} reverse(f32[3,256,4,128]{3,1,2,0:T(8,128)} %copy.79), dimensions={1} | reverse | bytes 3145728 | tf_op jit(solution)/shard_map/jit(_flip)/rev | solution.py:74
  236.1 5.3 fusion.11
  242.7 10.9 %while.27 = (s32[]{:T(128)}, f32[3,4,64,128]{3,2,1,0:T(8,128)S(1)}, f32[4,3,4,64,128]{4,3,2,0,1:T(8,128)}, f32[4,3,4,64]{3,2,0,1:T(4,128)}, f32[4,3,4,64,128]{4,3,2,1,0:T(8,128)}, /*index=5*/s32[]{:T(128)}, s32[]{:T(128)}) while((s32[]{:T(128)}, f32[3,4,64,128]{3,2,1,0:T(8,128)S(1)}, f32[4,3,4,64,128]{4,3,2,0,1:T(8,128)}, ...), condition=%wide.region_6.7_spmd.clone, body=%wide.region_5.6_spmd.clone.sunk | while | flops 393219 | bytes 1975904 | solution.py:54
  253.6 3.6 fusion.30
  257.3 1.7 add_bitcast_fusion
  260.2 10.4 %rev.21 = f32[3,256,4,128]{3,1,2,0:T(8,128)S(1)} reverse(f32[3,256,4,128]{3,1,2,0:T(8,128)} %bitcast.93), dimensions={1} | reverse | bytes 3145728 | tf_op jit(solution)/shard_map/jit(_flip)/rev | solution.py:77
  271.7 2.2 copy.97
  273.9 22.4 %all-gather.23.cloned.1.call-done = bf16[512,2048]{1,0:T(8,128)(2,1)} async-done(((bf16[512,256]{1,0:T(8,128)(2,1)}), bf16[512,2048]{1,0:T(8,128)(2,1)}) %all-gather.23.cloned.1.call-update) | async-done | bytes 2097168 | tf_op jit(solution)/shard_map/all_gather | solution.py:164
  296.3 8.1 %convolution_convert_fusion = bf16[768,2048]{1,0:T(8,128)(2,1)} fusion(bf16[512,2048]{1,0:T(8,128)(2,1)} %all-gather.23.cloned.1.call-done, f32[96,8,4,128]{3,2,1,0:T(4,128)} %bitcast.99, bf16[2048,512]{1,0:T(8,128)(2,1)} %all-gather.21.cloned.1.call-done, bf16[768,2048]{1,0:T(8,128)(2,1)S(1)} %copy-done.2, f32[2048]{0:T(1024)S(1)} %convert_element_type.115, ...), kind=kOutput, calls=%fused_computation.19 | convolution fusion | flops 3232235520 | bytes 12069888 | tf_op jit(solution)/shard_map/dot_general | solution.py:118
  306.8 21.9 %all-reduce.4.cloned.1.call-done = bf16[768,2048]{1,0:T(8,128)(2,1)} async-done(((bf16[768,2048]{1,0:T(8,128)(2,1)}), bf16[768,2048]{1,0:T(8,128)(2,1)}) %all-reduce.4.cloned.1.call-update) | async-done | bytes 3145744 | tf_op jit(solution)/shard_map/psum | solution.py:167
  328.6 5.1 fusion
  333.7 94.5 %all-gather.25.cloned.1.call-done = bf16[2048,1536]{1,0:T(8,128)(2,1)} async-done(((bf16[256,1536]{1,0:T(8,128)(2,1)}), bf16[2048,1536]{1,0:T(8,128)(2,1)}) %all-gather.25.cloned.1.call-update) | async-done | bytes 6291472 | tf_op jit(solution)/shard_map/all_gather | solution.py:176
  428.2 9.0 %convolution_convert_fusion.2 = bf16[768,1536]{1,0:T(8,128)(2,1)S(1)} fusion(bf16[2048,1536]{1,0:T(8,128)(2,1)} %all-gather.25.cloned.1.call-done, bf16[768,2048]{1,0:T(8,128)(2,1)} %get-tuple-element.166, f32[2048]{0:T(1024)S(1)} %convert_element_type.133, f32[768]{0:T(1024)S(1)} %add_rsqrt_fusion.1), kind=kOutput, calls=%fused_computation.21 | convolution fusion | flops 4839309312 | bytes 11807744 | tf_op jit(solution)/shard_map/dot_general | solution.py:111
  437.2 3.0 convert.11
  440.2 87.0 %all-gather.27.cloned.1.call-done = bf16[2048,1536]{1,0:T(8,128)(2,1)} async-done(((bf16[256,1536]{1,0:T(8,128)(2,1)}), bf16[2048,1536]{1,0:T(8,128)(2,1)}) %all-gather.27.cloned.1.call-update) | async-done | bytes 6291472 | tf_op jit(solution)/shard_map/all_gather | solution.py:177
  527.1 8.2 %convolution_convert_fusion.1 = bf16[768,1536]{1,0:T(8,128)(2,1)S(1)} fusion(bf16[2048,1536]{1,0:T(8,128)(2,1)} %all-gather.27.cloned.1.call-done, bf16[768,2048]{1,0:T(8,128)(2,1)S(1)} %copy-done.3, f32[2048]{0:T(1024)S(1)} %convert_element_type.133, f32[768]{0:T(1024)S(1)} %add_rsqrt_fusion.1), kind=kOutput, calls=%fused_computation.20 | convolution fusion | flops 4839309312 | bytes 11807744 | tf_op jit(solution)/shard_map/dot_general | solution.py:111
  536.0 1.9 copy-done
  537.9 5.3 multiply_convert_fusion
  543.2 83.7 %all-gather.29.cloned.1.call-done = bf16[1536,2048]{1,0:T(8,128)(2,1)} async-done(((bf16[1536,256]{1,0:T(8,128)(2,1)}), bf16[1536,2048]{1,0:T(8,128)(2,1)}) %all-gather.29.cloned.1.call-update) | async-done | bytes 6291472 | tf_op jit(solution)/shard_map/all_gather | solution.py:184
  626.9 9.0 %convolution_convert_fusion.3 = bf16[768,2048]{1,0:T(8,128)(2,1)} fusion(bf16[768,1536]{1,0:T(8,128)(2,1)} %bitcast.98, bf16[1536,2048]{1,0:T(8,128)(2,1)} %all-gather.29.cloned.1.call-done), kind=kOutput, calls=%fused_computation.22 | convolution fusion | flops 4833411072 | bytes 11796480 | tf_op jit(solution)/shard_map/dot_general | solution.py:118
  635.9 11.8 %reduce-scatter.2.cloned.1.call-done = bf16[768,1024]{1,0:T(8,128)(2,1)} async-done(((bf16[768,2048]{1,0:T(8,128)(2,1)}), bf16[768,1024]{1,0:T(8,128)(2,1)}) %reduce-scatter.2.cloned.1.call-update) | async-done | bytes 1572880 | tf_op jit(solution)/shard_map/reduce_scatter | solution.py:186
  647.7 3.2 add_convert_fusion
  (129 shorter events, 44.7 us)
Async XLA Ops:
  6.5 4.8 copy-start.15
  6.5 4.8 copy-start.22
  6.5 16.2 %all-gather.11.cloned.1.call-start = ((), (), s32[]{:S(2)}) async-start(), calls=%async_computation.1 | async-start | bytes 4718592 | tf_op jit(solution)/shard_map/all_gather | solution.py:140
  7.3 55.0 %all-gather.17.cloned.1.call-start = ((), (), s32[]{:S(2)}) async-start(), calls=%async_computation.4 | async-start | bytes 1179648 | tf_op jit(solution)/shard_map/all_gather | solution.py:149
  8.0 95.4 %all-gather.19.cloned.1.call-start = ((), (), s32[]{:S(2)}) async-start(), calls=%async_computation.5 | async-start | bytes 1179648 | tf_op jit(solution)/shard_map/all_gather | solution.py:146
  8.7 135.7 %all-gather.15.cloned.1.call-start = ((), (), s32[]{:S(2)}) async-start(), calls=%async_computation.3 | async-start | bytes 1179648 | tf_op jit(solution)/shard_map/all_gather | solution.py:145
  9.3 186.2 %all-gather.13.cloned.1.call-start = ((), (), s32[]{:S(2)}) async-start(), calls=%async_computation.2 | async-start | bytes 2359296 | tf_op jit(solution)/shard_map/all_gather | solution.py:147
  9.9 264.0 %all-gather.21.cloned.1.call-start = ((), (), s32[]{:S(2)}) async-start(), calls=%async_computation.6 | async-start | bytes 2359296 | tf_op jit(solution)/shard_map/all_gather | solution.py:148
  10.5 285.8 %all-gather.23.cloned.1.call-start = ((), (), s32[]{:S(2)}) async-start(), calls=%async_computation.7 | async-start | bytes 2359296 | tf_op jit(solution)/shard_map/all_gather | solution.py:164
  11.2 317.4 %all-reduce.4.cloned.1.call-start = ((), (), s32[]{:S(2)}) async-start(), calls=%async_computation.8 | async-start | bytes 6291456 | tf_op jit(solution)/shard_map/psum | solution.py:167
  11.8 50.5 %copy-start.20 = (f32[768,256]{1,0:T(8,128)S(1)}, f32[768,256]{1,0:T(8,128)}, u32[]{:S(2)}) copy-start(f32[768,256]{1,0:T(8,128)} %param.29) | copy-start | bytes 2359300
  11.8 50.5 %copy-start.21 = (f32[256]{0:T(256)S(1)}, f32[256]{0:T(256)}, u32[]{:S(2)}) copy-start(f32[256]{0:T(256)} %param.28) | copy-start | bytes 3076
  25.3 170.2 %copy-start.17 = (f32[768]{0:T(1024)}, f32[768]{0:T(1024)S(1)}, u32[]{:S(2)}) copy-start(f32[768]{0:T(1024)S(1)} %add_rsqrt_fusion.2) | copy-start | bytes 9220
  66.8 1.2 copy-start.4
  112.6 1.1 copy-start.5
  151.3 1.6 copy-start.12
  161.6 3.8 copy-start.6
  161.6 3.8 copy-start.10
  161.6 3.8 copy-start.11
  168.0 1.1 copy-start.1
  218.9 2.5 copy-start.8
  223.2 1.4 copy-start.7
  253.6 3.7 copy-start.9
  270.7 0.6 copy-start.19
  271.2 25.1 %copy-start.18 = (f32[768]{0:T(1024)S(1)}, f32[768]{0:T(1024)}, u32[]{:S(2)}) copy-start(f32[768]{0:T(1024)} %copy-done.17) | copy-start | bytes 9220
  271.7 24.6 %copy-start.2 = (bf16[768,2048]{1,0:T(8,128)(2,1)S(1)}, bf16[768,2048]{1,0:T(8,128)(2,1)}, u32[]{:S(2)}) copy-start(bf16[768,2048]{1,0:T(8,128)(2,1)} %all-gather.11.cloned.1.call-done) | copy-start | bytes 9437188
  304.4 2.1 copy-start.16
  304.4 2.2 copy-start.14
  304.5 2.2 copy-start.13
  304.5 123.7 %all-gather.25.cloned.1.call-start = ((), (), s32[]{:S(2)}) async-start(), calls=%async_computation.9 | async-start | bytes 7077888 | tf_op jit(solution)/shard_map/all_gather | solution.py:176
  305.2 221.9 %all-gather.27.cloned.1.call-start = ((), (), s32[]{:S(2)}) async-start(), calls=%async_computation.10 | async-start | bytes 7077888 | tf_op jit(solution)/shard_map/all_gather | solution.py:177
  305.8 321.1 %all-gather.29.cloned.1.call-start = ((), (), s32[]{:S(2)}) async-start(), calls=%async_computation.11 | async-start | bytes 7077888 | tf_op jit(solution)/shard_map/all_gather | solution.py:184
  306.5 341.2 %reduce-scatter.2.cloned.1.call-start = ((), (), s32[]{:S(2)}) async-start(), calls=%async_computation.12 | async-start | bytes 4718592 | tf_op jit(solution)/shard_map/reduce_scatter | solution.py:186
  437.2 90.0 %copy-start.3 = (bf16[768,2048]{1,0:T(8,128)(2,1)S(1)}, bf16[768,2048]{1,0:T(8,128)(2,1)}, u32[]{:S(2)}) copy-start(bf16[768,2048]{1,0:T(8,128)(2,1)} %get-tuple-element.166) | copy-start | bytes 9437188
  535.3 2.6 copy-start
Sparse Core Ops, SparseCore 0:
  8.9 13.8 all-gather.10
  24.9 37.3 all-gather.16
  64.4 38.9 all-gather.18
  105.4 38.9 all-gather.14
  146.4 49.0 all-gather.12
  197.5 47.6 all-gather.20
  247.2 49.0 all-gather.22
  304.5 24.0 all-reduce.3
  330.8 97.3 all-gather.24
  430.2 96.8 all-gather.26
  529.2 97.6 all-gather.28
  636.0 11.6 reduce-scatter.1
where the time goes:
time: 669 us; the launch traced here: 658 us
  waiting for transfers between devices  463 us (69%)
  matrix products  76 us (11%)
  local copies, waits for them, and re-layouts  58.4 us (9%)
  other arithmetic  45.5 us (7%)
  between operations  14.5 us (2%)
    all_gather x1, waiting for transfers between devices, local(): lax.all_gather(up_linear_weight, 'fs', axis=0, tiled=True)  94.5 us
    all_gather x1, waiting for transfers between devices, local(): lax.all_gather(up_gating_weight, 'fs', axis=0, tiled=True)  87 us
    all_gather x1, waiting for transfers between devices, local(): lax.all_gather(down_projection_weight, 'fs', axis=1, tiled=True)  83.7 us
    all_gather x1, waiting for transfers between devices, local(): lax.all_gather(decay_projection_weight, 'fs', axis=0, tiled=True)  37 us
    all_gather x1, waiting for transfers between devices, local(): lax.all_gather(key_projection_weight, 'fs', axis=0, tiled=True)  35.2 us
    dot_general x6, matrix products, fold_rows(): jnp.dot(source, weight_piece, preferred_element_type=jnp.float32)  32.4 us
    all_gather x1, waiting for transfers between devices, local(): lax.all_gather(query_projection_weight, 'fs', axis=0, tiled=True)  30.1 us
    all_gather x1, waiting for transfers between devices, local(): lax.all_gather(value_projection_weight, 'fs', axis=0, tiled=True)  22.6 us
  transfers between devices with their start and end apart: 12, of which 11 were waited for; matrix products, arithmetic and copies ran while one was open for 23% of the time, Pallas kernels for 0%

commit v1 on v0

v1 whole, which is shorter than its diff:
```python
import functools
import jax
import jax.numpy as jnp
from jax import lax
from jax.experimental import pallas as pl
from jax.experimental.pallas import tpu as pltpu
from jax.sharding import PartitionSpec as P

KEY_DIM = 64
VALUE_DIM = 128
BLOCK = 64
SEQ_LEN = 256
CHUNK = 256

norm_eps = 1e-06
fading_sharpness = 16.0
F32 = jnp.float32
BF16 = jnp.bfloat16


class Gather:
    def __init__(self, n, shared, own, full, recv, send):
        self.n, self.outer, self.shared = n, n // 2, shared
        self.own, self.full, self.recv, self.send = own, full, recv, send
        self.rows = own.shape[0]
        self.rep = lax.axis_index("rep")
        self.me = lax.axis_index("fs")
        self.hi, self.lo = self.me // 2, lax.rem(self.me, 2)
        self.half = self.rep if shared else 0

    def piece(self, ref, shard, half):
        rows = self.rows // 2 if self.shared else self.rows
        base = half * rows if shard is None else shard * self.rows + half * rows
        return ref.at[pl.ds(pl.multiple_of(base, rows), rows)]

    def local(self, sem):
        span = pl.ds(pl.multiple_of(self.me * self.rows, self.rows), self.rows)
        return pltpu.make_async_copy(self.own, self.full.at[span], sem)

    def copy(self, shard, half, slot, target, own=False):
        there = self.piece(self.full, shard, half)
        return pltpu.make_async_remote_copy(
            src_ref=self.piece(self.own, None, half) if own else there,
            dst_ref=there,
            send_sem=self.send.at[slot],
            recv_sem=self.recv.at[shard, half],
            device_id=target,
            device_id_type=pl.DeviceIdType.MESH,
        )

    def pair(self):
        return {"fs": self.hi * 2 + 1 - self.lo}

    def other(self):
        return {"rep": 1 - self.rep}

    def back(self, d, lo):
        return lax.rem(self.hi - d + self.outer, self.outer) * 2 + lo

    def start_outer(self):
        for d in range(1, self.outer):
            target = lax.rem(self.hi + d, self.outer) * 2 + self.lo
            self.copy(self.me, self.half, d - 1, {"fs": target}, own=True).start()

    def start_pair(self):
        self.copy(self.me, self.half, self.outer - 1, self.pair(), own=True).start()

    def outer_event(self, d):
        shard = self.back(d, self.lo)
        self.copy(shard, self.half, 0, self.pair()).wait_recv()
        self.copy(shard, self.half, self.outer - 1 + d, self.pair()).start()
        if self.shared:
            self.copy(shard, self.half, 2 * self.outer - 1 + d - 1, self.other()).start()

    def pair_event(self, d):
        shard = self.back(d, 1 - self.lo)
        self.copy(shard, self.half, 0, self.pair()).wait_recv()
        if self.shared:
            self.copy(shard, self.half, 3 * self.outer - 2 + d, self.other()).start()

    def rep_events(self):
        if self.shared:
            for d in range(1, self.outer):
                self.copy(self.back(d, self.lo), 1 - self.half, 0, self.other()).wait_recv()
            for d in range(self.outer):
                self.copy(self.back(d, 1 - self.lo), 1 - self.half, 0, self.other()).wait_recv()

    def finish(self):
        for slot in range((4 if self.shared else 2) * self.outer - (2 if self.shared else 1)):
            self.copy(self.me, self.half, slot, self.pair()).wait_send()


def greet(n):
    me, rep = lax.axis_index("fs"), lax.axis_index("rep")
    hi, lo, outer = me // 2, lax.rem(me, 2), n // 2
    barrier = pltpu.get_barrier_semaphore()
    targets = [{"fs": lax.rem(hi + d, outer) * 2 + lo} for d in range(1, outer)]
    targets += [{"fs": hi * 2 + 1 - lo}, {"rep": 1 - rep}, {"tp": 1 - lax.axis_index("tp")}]
    for target in targets:
        pl.semaphore_signal(barrier, inc=1, device_id=target, device_id_type=pl.DeviceIdType.MESH)
    pl.semaphore_wait(barrier, len(targets))


SHARED = (True, False, True, False)


def matmul(left, right):
    return jnp.dot(left, right, preferred_element_type=F32)


def matmul_t(left, right):
    return lax.dot_general(left, right, (((1,), (1,)), ((), ())), preferred_element_type=F32)


def matmul_0(left, right):
    return lax.dot_general(left, right, (((0,), (0,)), ((), ())), preferred_element_type=F32)


def silu(x):
    return x / (1.0 + jnp.exp(-x))


def scaled_rows(x, gain):
    return (x * lax.rsqrt(jnp.mean(x * x, axis=-1, keepdims=True) + norm_eps) * gain).astype(BF16)


def attend(rows, proj, decay, mixed, head_gain, keys, values):
    blocks = SEQ_LEN // BLOCK
    row = lax.broadcasted_iota(jnp.int32, (SEQ_LEN, SEQ_LEN), 0)
    column = lax.broadcasted_iota(jnp.int32, (SEQ_LEN, SEQ_LEN), 1)
    tri = jnp.where((row >= column) & (row // BLOCK == column // BLOCK), 1.0, 0.0).astype(BF16)
    small_row = lax.broadcasted_iota(jnp.int32, (BLOCK, BLOCK), 0)
    small_column = lax.broadcasted_iota(jnp.int32, (BLOCK, BLOCK), 1)
    lane = lax.broadcasted_iota(jnp.int32, (1, 2 * KEY_DIM), 1)
    for pair in range(keys // (2 * KEY_DIM)):
        at = pair * 2 * KEY_DIM
        span = slice(at, at + 2 * KEY_DIM)
        ld = decay[rows, span]
        high = ld.astype(BF16)
        low = (ld - high.astype(F32)).astype(BF16)
        cum = matmul(tri, high) + matmul(tri, low)
        q = proj[rows, span].astype(F32) * KEY_DIM ** (-0.5)
        k = proj[rows, keys + at : keys + at + 2 * KEY_DIM].astype(F32)
        parts = []
        for b in range(blocks):
            inside = slice(b * BLOCK, (b + 1) * BLOCK)
            c, x, y = cum[inside], q[inside], k[inside]
            e = c - ld[inside]
            total = c[BLOCK - 1 : BLOCK]
            r = total - e
            parts.append(
                (
                    (x * jnp.exp(c)).astype(BF16),
                    y * jnp.exp(-c),
                    y * jnp.exp(total - c),
                    (x * jnp.exp(r)).astype(BF16),
                    y * jnp.exp(-r),
                    y * jnp.exp(e),
                    jnp.exp(total),
                )
            )
        for h in range(2):
            mask = (lane // KEY_DIM) == h

            def only(z):
                return jnp.where(mask, z, 0.0).astype(BF16)

            head = pair * 2 + h
            at_v = 2 * keys + head * VALUE_DIM
            v = proj[rows, at_v : at_v + VALUE_DIM]
            gate = proj[rows, at_v + values : at_v + values + VALUE_DIM].astype(F32)
            outs = []
            for b in range(blocks):
                qf, kf, _, qb, kb, _, _ = parts[b]
                scores = jnp.where(small_row >= small_column, matmul_t(qf, only(kf)), 0.0)
                scores += jnp.where(small_row <= small_column, matmul_t(qb, only(kb)), 0.0)
                outs.append(matmul(scores.astype(BF16), v[b * BLOCK : (b + 1) * BLOCK]))
            state = None
            for b in range(blocks):
                if state is not None:
                    outs[b] += matmul_t(parts[b][0], state.astype(BF16))
                if b < blocks - 1:
                    update = matmul_0(v[b * BLOCK : (b + 1) * BLOCK], only(parts[b][2]))
                    state = update if state is None else state * parts[b][6] + update
            state = None
            for b in reversed(range(blocks)):
                if state is not None:
                    outs[b] += matmul_t(parts[b][3], state.astype(BF16))
                if b > 0:
                    update = matmul_0(v[b * BLOCK : (b + 1) * BLOCK], only(parts[b][5]))
                    state = update if state is None else state * parts[b][6] + update
            y = jnp.concatenate(outs, axis=0)
            y = y * lax.rsqrt(jnp.mean(y * y, axis=-1, keepdims=True) + norm_eps) * head_gain
            mixed[rows, head * VALUE_DIM : (head + 1) * VALUE_DIM] = (y * silu(gate)).astype(BF16)


def layer_kernel(n, keys, values, *refs):
    tokens, added, shift, gain_one, gain_two, head_gain, conv = refs[:7]
    owns, out = refs[7:11], refs[11]
    fulls = refs[12:16]
    tok, normed, terms, theirs, proj, decay, mixed, arrived = refs[16:24]
    recvs, sends = refs[24:28], refs[28:32]
    local_sem, tp_send, tp_recv = refs[32:35]
    t = lax.axis_index("tp")
    count, share = tokens.shape
    units = conv.shape[1]
    mine = pl.ds(pl.multiple_of(t * share, share), share)
    greet(n)

    def swap(source, target, slot):
        return pltpu.make_async_remote_copy(
            src_ref=source,
            dst_ref=target,
            send_sem=tp_send.at[slot],
            recv_sem=tp_recv.at[slot],
            device_id={"tp": 1 - t},
            device_id_type=pl.DeviceIdType.MESH,
        )

    token_swap = swap(tokens, tok.at[:, mine], 0)
    token_swap.start()
    gathers = [Gather(n, *entry) for entry in zip(SHARED, owns, fulls, recvs, sends)]
    a, m, u, d = gathers
    outer = a.outer
    for g in gathers:
        g.start_outer()
    a.start_pair()
    m.start_pair()
    locals_ = [g.local(local_sem.at[i]) for i, g in enumerate(gathers)]
    locals_.append(pltpu.make_async_copy(tokens, tok.at[:, mine], local_sem.at[4]))
    for c in locals_:
        c.start()
    for c in locals_:
        c.wait()
    token_swap.wait()
    step = 64

    @pl.loop(0, count // step)
    def _(i):
        rows = pl.ds(pl.multiple_of(i * step, step), step)
        normed[rows] = scaled_rows(tok[rows].astype(F32), gain_one[...])

    def through(g, first, last):
        for k in range(first, last):
            g.outer_event(k)
            g.pair_event(k)

    a.pair_event(0)
    through(a, 1, outer)
    u.start_pair()
    m.pair_event(0)
    through(m, 1, outer)
    u.pair_event(0)
    a.rep_events()
    attention_full, mixer_full, up_full, down_full = fulls

    @pl.loop(0, (2 * keys + 2 * values) // CHUNK)
    def _(j):
        cols = pl.ds(pl.multiple_of(j * CHUNK, CHUNK), CHUNK)
        proj[:, cols] = matmul(normed[...], attention_full[:, cols]).astype(BF16)

    z = matmul(normed[...], attention_full[:, 2 * keys + 2 * values :]) + shift[...]
    log_sigmoid = jnp.minimum(z, 0.0) - jnp.log(1.0 + jnp.exp(-jnp.abs(z)))
    decay[...] = log_sigmoid / fading_sharpness + added[...]
    half = (outer + 1) // 2
    through(u, 1, half + 1)
    d.start_pair()

    @pl.loop(0, count // SEQ_LEN)
    def _(s):
        rows = pl.ds(pl.multiple_of(s * SEQ_LEN, SEQ_LEN), SEQ_LEN)
        attend(rows, proj, decay, mixed, head_gain[...], keys, values)

    through(u, half + 1, outer)
    d.pair_event(0)
    swaps = []
    for part in range(2):

        @pl.loop(0, share // CHUNK)
        def _(j):
            cols = pl.ds(pl.multiple_of(part * share + j * CHUNK, CHUNK), CHUNK)
            terms[:, cols] = matmul_t(mixed[...], mixer_full[cols]).astype(BF16)

        cols = pl.ds(part * share, share)
        swaps.append(swap(terms.at[:, cols], theirs.at[:, cols], 1 + part))
        swaps[-1].start()
    for c in swaps:
        c.wait()

    @pl.loop(0, count // step)
    def _(i):
        rows = pl.ds(pl.multiple_of(i * step, step), step)
        summed = terms[rows].astype(F32) + theirs[rows].astype(F32)
        after = (tok[rows].astype(F32) + summed).astype(BF16)
        tok[rows] = after
        normed[rows] = scaled_rows(after.astype(F32), gain_two[...])

    through(d, 1, outer - 1)
    u.rep_events()
    if outer > 1:
        d.outer_event(outer - 1)
    place = lax.rem(lax.broadcasted_iota(jnp.int32, (count, 1), 0), SEQ_LEN)

    def smooth(x, taps, bias):
        x = x.astype(BF16).astype(F32)
        before = jnp.where(place == 0, 0.0, pltpu.roll(x, 1, 0))
        behind = jnp.where(place == SEQ_LEN - 1, 0.0, pltpu.roll(x, count - 1, 0))
        return bias + before * taps[0:1] + x * taps[1:2] + behind * taps[2:3]

    @pl.loop(0, units // CHUNK)
    def _(j):
        cols = pl.ds(pl.multiple_of(j * CHUNK, CHUNK), CHUNK)
        gate_cols = pl.ds(pl.multiple_of(units + j * CHUNK, CHUNK), CHUNK)
        table = conv[:, cols]
        linear = smooth(matmul(normed[...], up_full[:, cols]), table[0:3], table[6:7])
        gate = smooth(matmul(normed[...], up_full[:, gate_cols]), table[3:6], table[7:8])
        proj[:, cols] = (linear * silu(gate)).astype(BF16)

    if outer > 1:
        d.pair_event(outer - 1)
    for part in range(2):
        base = lax.rem(t + 1 + part, 2) * share

        @pl.loop(0, share // CHUNK)
        def _(j):
            cols = pl.ds(pl.multiple_of(part * share + j * CHUNK, CHUNK), CHUNK)
            units_rows = pl.ds(pl.multiple_of(base + j * CHUNK, CHUNK), CHUNK)
            terms[:, cols] = matmul_t(proj[:, :units], down_full[units_rows]).astype(BF16)

        if part == 0:
            last = swap(terms.at[:, pl.ds(0, share)], arrived, 3)
            last.start()
    last.wait()

    @pl.loop(0, count // step)
    def _(i):
        rows = pl.ds(pl.multiple_of(i * step, step), step)
        summed = terms[rows, share:].astype(F32) + arrived[rows].astype(F32)
        out[rows] = (tok[rows, mine].astype(F32) + summed).astype(BF16)

    for g in gathers:
        g.finish()


def local(
    n,
    tokens,
    first_norm_gain,
    query_projection_weight,
    key_projection_weight,
    value_projection_weight,
    output_gate_weight,
    decay_projection_weight,
    fading_shift_vector,
    added_fading_exponent,
    per_head_gain,
    mixer_result_matrix,
    second_norm_gain,
    up_linear_weight,
    up_gating_weight,
    depthwise_taps,
    depthwise_bias,
    down_projection_weight,
):
    attention_weight = jnp.concatenate(
        [
            query_projection_weight,
            key_projection_weight,
            value_projection_weight,
            output_gate_weight,
            decay_projection_weight,
        ],
        axis=1,
    )
    up_weight = jnp.concatenate([up_linear_weight, up_gating_weight], axis=1)
    shards = (attention_weight, mixer_result_matrix.T, up_weight, down_projection_weight.T)
    keys, values = query_projection_weight.shape[1], value_projection_weight.shape[1]
    units = up_linear_weight.shape[1]
    conv = jnp.concatenate(
        [depthwise_taps.reshape(-1, units), depthwise_bias], axis=0
    ).astype(F32)
    count, share = tokens.shape
    wide = max(units, 2 * keys + 2 * values)
    outer = n // 2
    anywhere = pl.BlockSpec(memory_space=pl.ANY)
    vmem = pl.BlockSpec(memory_space=pltpu.VMEM)
    return pl.pallas_call(
        functools.partial(layer_kernel, n, keys, values),
        out_shape=jax.ShapeDtypeStruct(tokens.shape, BF16),
        in_specs=[anywhere] + [vmem] * 6 + [anywhere] * 4,
        out_specs=vmem,
        scratch_shapes=[pltpu.VMEM((n * s.shape[0], s.shape[1]), BF16) for s in shards]
        + [
            pltpu.VMEM((count, 2 * share), BF16),
            pltpu.VMEM((count, 2 * share), BF16),
            pltpu.VMEM((count, 2 * share), BF16),
            pltpu.VMEM((count, 2 * share), BF16),
            pltpu.VMEM((count, wide), BF16),
            pltpu.VMEM((count, keys), F32),
            pltpu.VMEM((count, values), BF16),
            pltpu.VMEM((count, share), BF16),
        ]
        + [pltpu.SemaphoreType.DMA((n, 2)) for s in shards]
        + [pltpu.SemaphoreType.DMA((4 * outer,)) for s in shards]
        + [
            pltpu.SemaphoreType.DMA((5,)),
            pltpu.SemaphoreType.DMA((4,)),
            pltpu.SemaphoreType.DMA((4,)),
        ],
        compiler_params=pltpu.CompilerParams(
            collective_id=0, has_side_effects=True, vmem_limit_bytes=67043328
        ),
        name="layer",
    )(
        tokens,
        added_fading_exponent,
        fading_shift_vector.reshape(1, -1),
        first_norm_gain.astype(F32).reshape(1, -1),
        second_norm_gain.astype(F32).reshape(1, -1),
        per_head_gain.astype(F32).reshape(1, -1),
        conv,
        *shards,
    )


def solution(mesh):
    return jax.shard_map(
        functools.partial(local, mesh.shape["fs"]),
        mesh=mesh,
        in_specs=(
            P(("rep", "fs"), "tp"),
            P(),
            P("fs", "tp"),
            P("fs", "tp"),
            P("fs", "tp"),
            P("fs", "tp"),
            P("fs", "tp"),
            P("tp"),
            P(("rep", "fs"), "tp"),
            P(),
            P("tp", "fs"),
            P(),
            P("fs", "tp"),
            P("fs", "tp"),
            P(None, None, "tp"),
            P(None, "tp"),
            P("tp", "fs"),
        ),
        out_specs=P(("rep", "fs"), "tp"),
        check_vma=False,
    )
```

time: 669 us -> 313 us (0.47); the launches traced: 658 us -> 312 us
  waiting for transfers between devices: 463 us -> 0 us
  Pallas kernels: 0 us -> 295 us
  matrix products: 76 us -> 0 us
  local copies, waits for them, and re-layouts: 58.4 us -> 11.2 us
  other arithmetic: 45.5 us -> 6.54 us
  between operations: 14.5 us -> 0.03 us
    all_gather x10 -> x0, waiting for transfers between devices: 423 us -> none  [the longest x1 94.5 us: local(): lax.all_gather(up_linear_weight, 'fs', axis=0, tiled=True)]
    pallas_call x0 -> x1, Pallas kernels: none -> 295 us  [local(): pl.pallas_call(functools.partial(layer_kernel, n, keys, values), out_shap...]
    dot_general x16 -> x0, matrix products: 76 us -> none  [the longest x6 32.4 us: fold_rows(): jnp.dot(source, weight_piece, preferred_element_type=jnp.float32)]
    rev x5 -> x0, local copies, waits for them, and re-layouts: 25.5 us -> none  [the longest x1 10.4 us: mixer_heads(): attention = forward + jnp.flip(backward, 1)]
    psum x1 -> x0, waiting for transfers between devices: 21.9 us -> none  [local(): lax.psum(mixer_terms.astype(jnp.bfloat16), 'tp').astype(jnp.float32)]
    reduce_scatter x1 -> x0, waiting for transfers between devices: 11.8 us -> none  [local(): lax.psum_scatter(channel_terms.astype(jnp.bfloat16), 'tp', scatter_dimens...]
    add x8 -> x0, other arithmetic: 9.76 us -> none  [advance(): return (factor[..., None] * running + update, running)]
    reshape x8 -> x1, local copies, waits for them, and re-layouts: 8.63 us -> 0.03 us  [local(): depthwise_taps.reshape(-1, units)]
  transfers between devices with their start and end apart: 12 -> 0, of which waited for: 11 -> 0; matrix products, arithmetic and copies ran while one was open for 23% -> 0% of each run, Pallas kernels for 0% -> 0%
where the time goes in v1:
time: 313 us; the launch traced here: 312 us
  Pallas kernels  295 us (94%)
  local copies, waits for them, and re-layouts  11.2 us (4%)
  other arithmetic  6.54 us (2%)
    pallas_call x1, Pallas kernels, local(): pl.pallas_call(functools.partial(layer_kernel, n, keys, values), out_shap...  295 us
    unnamed x22, local copies, waits for them, and re-layouts  10.5 us

profile of v1, /device:TPU:25, one launch (start us, length us, event | category | flops | bytes accessed | tf_op | source)
XLA Modules:
  0.0 312.4 jit_solution(10115063050742854379)
XLA Ops:
  0.0 0.0 copy-start.2
  0.0 0.0 copy-start.5
  0.0 0.0 copy-start.4
  0.0 1.3 bitcast_convert_fusion.refs_5_
  1.3 1.3 reshape.29
  2.6 1.3 reshape.31
  3.9 0.7 copy.21
  4.6 1.3 maximum_convert_fusion.refs_6_
  6.0 0.0 copy-start.3
  6.0 1.8 copy.22
  7.8 0.0 copy-start.6
  7.8 0.0 copy-start
  7.8 0.0 copy-start.1
  7.8 2.4 copy.23
  10.2 0.0 copy-done.4
  10.2 0.7 constant_dynamic-update-slice_fusion.4
  10.9 0.0 copy-done.5
  10.9 0.7 constant_dynamic-update-slice_fusion.3
  11.6 0.0 copy-done.2
  11.6 0.7 constant_dynamic-update-slice_fusion.2
  12.3 0.0 copy-done.3
  12.3 0.8 constant_dynamic-update-slice_fusion.1
  13.1 0.0 copy-done.6
  13.1 0.7 constant_dynamic-update-slice_fusion.refs_7_
  13.8 0.0 copy-done
  13.8 0.0 copy-done.1
  13.8 1.4 pad_maximum_fusion.refs_9_
  15.1 294.6 %layer.1 = bf16[768,1024]{1,0:T(8,128)(2,1)} custom-call(bf16[768,1024]{1,0:T(8,128)(2,1)} %refs_0_.1, f32[768,256]{1,0:T(8,128)} %refs_1_.1, f32[1,256]{1,0:T(1,128)} %bitcast.12, f32[1,2048]{1,0:T(1,128)} %bitcast.10, f32[1,2048]{1,0:T(1,128)} %bitcast.11, f32[1,128]{1,0:T(1,128)} %bitcast_convert_fusion.refs_5_, f32[8,1536]{1,0:T(8,128)} %maximum_convert_fusion.refs_6_, ...), custom_call_target="tpu_custom_call" | custom-call | tf_op jit(solution)/shard_map/layer/pallas_call | solution.py:387
  309.7 2.7 copy.29
  (1 shorter events, 0.0 us)
Async XLA Ops:
  0.0 11.6 %copy-start.2 = (bf16[256,512]{1,0:T(8,128)(2,1)S(1)}, bf16[256,512]{1,0:T(8,128)(2,1)}, u32[]{:S(2)}) copy-start(bf16[256,512]{1,0:T(8,128)(2,1)} %param.21) | copy-start | bytes 786436
  0.0 10.9 %copy-start.5 = (bf16[256,256]{1,0:T(8,128)(2,1)S(1)}, bf16[256,256]{1,0:T(8,128)(2,1)}, u32[]{:S(2)}) copy-start(bf16[256,256]{1,0:T(8,128)(2,1)} %param.20) | copy-start | bytes 393220
  0.0 10.2 %copy-start.4 = (bf16[256,256]{1,0:T(8,128)(2,1)S(1)}, bf16[256,256]{1,0:T(8,128)(2,1)}, u32[]{:S(2)}) copy-start(bf16[256,256]{1,0:T(8,128)(2,1)} %param.19) | copy-start | bytes 393220
  6.0 6.4 %copy-start.3 = (bf16[256,512]{1,0:T(8,128)(2,1)S(1)}, bf16[256,512]{1,0:T(8,128)(2,1)}, u32[]{:S(2)}) copy-start(bf16[256,512]{1,0:T(8,128)(2,1)} %param.22) | copy-start | bytes 786436
  7.8 5.3 %copy-start.6 = (bf16[256,256]{1,0:T(8,128)(2,1)S(1)}, bf16[256,256]{1,0:T(8,128)(2,1)}, u32[]{:S(2)}) copy-start(bf16[256,256]{1,0:T(8,128)(2,1)} %param.23) | copy-start | bytes 393220
  7.8 6.0 %copy-start = (bf16[256,1536]{1,0:T(8,128)(2,1)S(1)}, bf16[256,1536]{1,0:T(8,128)(2,1)}, u32[]{:S(2)}) copy-start(bf16[256,1536]{1,0:T(8,128)(2,1)} %param.30) | copy-start | bytes 2359300
  7.8 6.0 %copy-start.1 = (bf16[256,1536]{1,0:T(8,128)(2,1)S(1)}, bf16[256,1536]{1,0:T(8,128)(2,1)}, u32[]{:S(2)}) copy-start(bf16[256,1536]{1,0:T(8,128)(2,1)} %param.29) | copy-start | bytes 2359300
